TPU v7x, 32 devices: a whole 2x2x4 slice. The times are simulated.
32 devices in a mesh: sp: 8 (over z, x), tp: 4 (over y, core).
Axes of the slice: x: 2, y: 2, z: 4, core: 2. Of those that a mesh axis runs over, the one named last changes fastest.
Arguments:
- residual_in: bfloat16 [1536, 2048], P('sp', 'tp'), may hold values from -6 to 6
- query_rows: bfloat16 [1536, 1024], P('sp', 'tp'), may hold values from -8 to 8
- key_rows: bfloat16 [1536, 1024], P('sp', 'tp'), may hold values from -8 to 8
- value_rows: bfloat16 [1536, 1024], P('sp', 'tp'), may hold values from -6 to 6
- map_weight: float32 [16], P('tp'), may hold values from 0.3 to 0.8
- head_gain: float32 [64], replicated, may hold values from 0.1 to 1.9
- out_proj: bfloat16 [1024, 2048], P(None, 'tp'), may hold values from -0.1875 to 0.1875
- norm_gain: float32 [2048], replicated, may hold values from 0.1 to 1.9
- route_ids: int32 [1536, 2], P('sp'), may hold values from 0 to 7, all different within a row; in each aligned block of 192 rows (0 to 191, 192 to 383, ...) at most 60 rows name the same one
- route_weights: float32 [1536, 2], P('sp'), may hold values from 0.2 to 1.2
- expert_gate: bfloat16 [8, 1024, 2048], P('sp', 'tp'), may hold values from -0.125 to 0.125
- expert_up: bfloat16 [8, 1024, 2048], P('sp', 'tp'), may hold values from -0.125 to 0.125
- expert_down: bfloat16 [8, 1024, 2048], P('sp', None, 'tp'), may hold values from -0.1875 to 0.1875
- shared_gate: bfloat16 [1024, 2048], P('tp'), may hold values from -0.125 to 0.125
- shared_up: bfloat16 [1024, 2048], P('tp'), may hold values from -0.125 to 0.125
- shared_down: bfloat16 [1024, 2048], P(None, 'tp'), may hold values from -0.1875 to 0.1875
Outputs:
- mixed_out: bfloat16 [1536, 2048], P('sp', 'tp')
Inputs may be any that keep to these rules, and one draw needn't show every extreme that they name: `route_ids`: each row names 2 different experts. Among the rows held by one index of sp no expert is named more than 60 times, and in every draw some expert is named exactly 60 times by the rows of some index of sp.
All inputs are finite; a program needn't handle non-finite values.
Results may differ from a plain program's by a relative error of at most 0.0095.
Values may be sent and summed in bfloat16 or wider, within the bound.
No kernel may reach another device: no remote copies, remote signals or barrier semaphores. Data moves between devices by JAX's collectives and lax.ppermute only.
A program may use at most 64 MiB of HBM per device.

v0:
```python
import jax
import jax.numpy as jnp
from jax import lax
from jax.sharding import PartitionSpec as P

epsilon = 1e-06
masked_score = -1e30


def rms_scale(values, gain_vec):
    squares = jnp.mean(values * values, axis=-1, keepdims=True)
    return values * lax.rsqrt(squares + epsilon) * gain_vec


def block_slots(route_block, experts_all, capacity):
    flat_ids = route_block.reshape(-1)
    one_hot = (flat_ids[:, None] == jnp.arange(experts_all, dtype=jnp.int32)[None, :]).astype(
        jnp.int32
    )
    earlier = jnp.cumsum(one_hot, axis=0) - one_hot
    position = jnp.sum(earlier * one_hot, axis=1)
    return (flat_ids * capacity + position).reshape(route_block.shape)


def body(
    residual_in,
    query_rows,
    key_rows,
    value_rows,
    map_weight,
    head_gain,
    out_proj,
    norm_gain,
    route_ids,
    route_weights,
    expert_gate,
    expert_up,
    expert_down,
    shared_gate,
    shared_up,
    shared_down,
):
    seq_dev = residual_in.shape[0]
    col_dev = residual_in.shape[1]
    heads_here = map_weight.shape[0]
    head_dim = head_gain.shape[0]
    half_dim = head_dim // 2
    topk_count = route_ids.shape[1]
    exp_here = expert_gate.shape[0]
    experts_all = exp_here * lax.axis_size("sp")
    capacity = 5 * seq_dev * topk_count // (4 * experts_all)
    score_scale = half_dim ** (-0.5)
    query_pos = lax.axis_index("sp") * seq_dev + jnp.arange(seq_dev, dtype=jnp.int32)
    query_heads = query_rows.reshape(seq_dev, heads_here, 2, half_dim)
    key_piece = lax.all_gather(key_rows, "sp", axis=0, tiled=True)
    value_piece = lax.all_gather(value_rows, "sp", axis=0, tiled=True)
    piece_len = key_piece.shape[0]
    key_heads = key_piece.reshape(piece_len, heads_here, 2, half_dim)
    value_heads = value_piece.reshape(piece_len, heads_here, head_dim)
    scores = (
        jnp.einsum("qhmd,khmd->mhqk", query_heads, key_heads, preferred_element_type=jnp.float32)
        * score_scale
    )
    key_pos = jnp.arange(piece_len, dtype=jnp.int32)
    visible = key_pos[None, :] <= query_pos[:, None]
    scores = jnp.where(visible, scores, masked_score)
    run_max = jnp.full((2, heads_here, seq_dev), masked_score, jnp.float32)
    new_max = jnp.maximum(run_max, jnp.max(scores, axis=-1))
    expo = jnp.where(visible, jnp.exp(scores - new_max[..., None]), 0.0)
    new_sum = jnp.sum(expo, axis=-1)
    product = jnp.einsum(
        "mhqk,khd->mhqd", expo.astype(jnp.bfloat16), value_heads, preferred_element_type=jnp.float32
    )
    summed = product / new_sum[..., None]
    diff_out = summed[0] - map_weight[:, None, None] * summed[1]
    head_out = rms_scale(diff_out, head_gain).astype(jnp.bfloat16)
    head_out = jnp.transpose(head_out, (1, 0, 2)).reshape(seq_dev, heads_here * head_dim)
    attn = jnp.dot(
        lax.all_gather(head_out, "tp", axis=1, tiled=True),
        out_proj,
        preferred_element_type=jnp.float32,
    )
    hidden_state = (residual_in.astype(jnp.float32) + attn).astype(jnp.bfloat16)
    full_rows = lax.all_gather(hidden_state, "tp", axis=1, tiled=True)
    normed = rms_scale(full_rows.astype(jnp.float32), norm_gain).astype(jnp.bfloat16)
    shared_gate_part = jnp.einsum(
        "rd,fd->rf", normed, shared_gate, preferred_element_type=jnp.float32
    )
    shared_up_part = jnp.einsum("rd,fd->rf", normed, shared_up, preferred_element_type=jnp.float32)
    shared_hidden = (jax.nn.silu(shared_gate_part) * shared_up_part).astype(jnp.bfloat16)
    slot_ids = block_slots(route_ids, experts_all, capacity)
    token_of = jnp.repeat(jnp.arange(seq_dev, dtype=jnp.int32), topk_count)
    slot_token = (
        jnp.full((experts_all * capacity,), seq_dev, jnp.int32)
        .at[slot_ids.reshape(-1)]
        .set(token_of)
    )
    own_cols = lax.dynamic_slice_in_dim(normed, lax.axis_index("tp") * col_dev, col_dev, 1)
    padded = jnp.concatenate([own_cols, jnp.zeros((1, col_dev), jnp.bfloat16)], axis=0)
    outgoing = jnp.take(padded, slot_token, axis=0).reshape(experts_all, capacity, col_dev)
    arrived = lax.all_to_all(outgoing, "sp", split_axis=0, concat_axis=1, tiled=True)
    arrived_rows = arrived.shape[1]
    pieces = lax.all_gather(arrived, "tp", axis=2, tiled=True)
    gate_add = jnp.einsum("erd,efd->erf", pieces, expert_gate, preferred_element_type=jnp.float32)
    up_add = jnp.einsum("erd,efd->erf", pieces, expert_up, preferred_element_type=jnp.float32)
    expert_hidden = (jax.nn.silu(gate_add) * up_add).astype(jnp.bfloat16)
    expert_flat = expert_hidden.reshape(exp_here * arrived_rows, expert_hidden.shape[2])
    pieces = (
        lax.all_gather(shared_hidden, "tp", axis=1, tiled=True),
        lax.all_gather(expert_flat, "tp", axis=1, tiled=True),
    )
    piece_width = pieces[0].shape[1]
    routed_piece = pieces[1].reshape(exp_here, arrived_rows, piece_width)
    shared_add = jnp.dot(pieces[0], shared_down, preferred_element_type=jnp.float32)
    expert_add = jnp.einsum(
        "erf,efd->erd", routed_piece, expert_down, preferred_element_type=jnp.float32
    )
    returned_rows = lax.all_to_all(
        expert_add.astype(jnp.bfloat16), "sp", split_axis=1, concat_axis=0, tiled=True
    )
    returned_flat = returned_rows.reshape(experts_all * capacity, col_dev)
    picked = (
        jnp.take(returned_flat, slot_ids.reshape(-1), axis=0)
        .reshape(seq_dev, topk_count, col_dev)
        .astype(jnp.float32)
    )
    routed = jnp.sum(picked * route_weights[:, :, None], axis=1)
    return (hidden_state.astype(jnp.float32) + shared_add + routed).astype(jnp.bfloat16)


def solution(mesh):
    in_specs = (
        P("sp", "tp"),
        P("sp", "tp"),
        P("sp", "tp"),
        P("sp", "tp"),
        P("tp"),
        P(),
        P(None, "tp"),
        P(),
        P("sp", None),
        P("sp", None),
        P("sp", "tp", None),
        P("sp", "tp", None),
        P("sp", None, "tp"),
        P("tp", None),
        P("tp", None),
        P(None, "tp"),
    )
    out_specs = P("sp", "tp")
    return jax.shard_map(body, mesh=mesh, in_specs=in_specs, out_specs=out_specs, check_vma=False)
```

profile of v0, /device:TPU:0, one launch (start us, length us, event | category | flops | bytes accessed | tf_op | source)
XLA Modules:
  0.0 206.6 jit_solution(2744693201549045714)
XLA Ops:
  6.5 0.9 copy.68
  7.4 0.1 eq.26
  7.6 0.1 reshape.160
  7.7 0.7 broadcast_multiply_fusion
  8.4 0.8 reduce-window.6
  9.3 0.2 slice_reduce_fusion
  9.5 0.1 copy.72
  9.6 0.1 mul.124
  9.8 0.1 reshape.188
  9.9 0.1 fusion.38
  10.1 2.9 %scatter_custom_fusion = s32[480]{0:T(512)S(1)} fusion(s32[384]{0:T(512)S(1)} %fusion.40, s32[384]{0:T(512)S(1)} %reshape.188, s32[]{:T(128)} %constant.26.clone.1), kind=kCustom, calls=%fused_computation.66 | custom fusion | bytes 1924 | tf_op jit(solution)/shard_map/scatter | solution.py:96
  13.0 0.2 iota_compare_fusion
  13.3 34.1 %all_gather.21 = bf16[1536,256]{1,0:T(8,128)(2,1)S(1)} all-gather(bf16[192,256]{1,0:T(8,128)(2,1)} %param.18), channel_id=1, replica_groups=mesh['sp'=8,'tp'=4] {'sp'}, dimensions={0}, use_global_device_ids=true | all-gather | bytes 884736 | tf_op jit(solution)/shard_map/all_gather | solution.py:55
  47.4 0.3 copy.61
  47.6 1.0 copy.60
  48.6 1.9 fusion
  50.5 0.0 copy-start.2
  50.5 4.4 %fusion.1 = (f32[2,4,192]{2,1,0:T(4,128)S(1)}, bf16[2,4,192,1536]{3,2,1,0:T(8,128)(2,1)}) fusion(f32[2,4,192,1536]{3,2,1,0:T(8,128)S(1)} %get-tuple-element.8, f32[2,4,192]{2,1,0:T(4,128)S(1)} %broadcast_maximum_fusion, pred[192,1536]{1,0:T(8,128)(4,1)S(1)} %iota_compare_fusion), kind=kLoop, calls=%fused_computation.6 | loop fusion | flops 14154240 | bytes 14462976 | tf_op jit(solution)/shard_map/reduce_sum | solution.py:70
  55.0 32.1 %all_gather.22 = bf16[1536,256]{1,0:T(8,128)(2,1)S(1)} all-gather(bf16[192,256]{1,0:T(8,128)(2,1)S(1)} %copy-done.2), channel_id=1, replica_groups=mesh['sp'=8,'tp'=4] {'sp'}, dimensions={0}, use_global_device_ids=true | all-gather | bytes 884736 | tf_op jit(solution)/shard_map/all_gather | solution.py:56
  87.1 0.3 copy.64
  87.4 0.0 copy-start.9
  87.4 0.0 copy-start.11
  87.4 4.0 %fusion.29 = f32[2,4,192,64]{2,3,0,1:T(8,128)S(1)} fusion(bf16[1536,4,64,1]{0,2,3,1:T(8,128)(2,1)S(1)} %bitcast.84, bf16[2,4,192,1536]{3,2,1,0:T(8,128)(2,1)} %get-tuple-element.6, f32[2,4,192]{2,0,1:T(2,128)S(1)} %copy.66), kind=kOutput, calls=%fused_computation.35 | convolution fusion | flops 302088192 | bytes 5904384 | tf_op jit(solution)/shard_map/mhqk,khd->mhqd/dot_general | solution.py:71
  91.5 0.1 multiply_reduce_fusion.1
  91.6 0.1 multiply_convert_fusion
  91.7 7.2 %all_gather.23 = bf16[192,1024]{0,1:T(8,128)(2,1)S(1)} all-gather(bf16[192,256]{0,1:T(8,128)(2,1)S(1)} %bitcast.85), channel_id=1, replica_groups=mesh['sp'=8,'tp'=4] {'tp'}, dimensions={1}, use_global_device_ids=true | all-gather | bytes 491520 | tf_op jit(solution)/shard_map/all_gather | solution.py:79
  98.9 1.1 fusion.23
  100.0 8.9 %all_gather.24 = bf16[192,2048]{1,0:T(8,128)(2,1)S(1)} all-gather(bf16[192,512]{1,0:T(8,128)(2,1)} %fusion.23), channel_id=1, replica_groups=mesh['sp'=8,'tp'=4] {'tp'}, dimensions={1}, use_global_device_ids=true | all-gather | bytes 983040 | tf_op jit(solution)/shard_map/all_gather | solution.py:84
  108.9 0.2 fusion.9
  109.2 0.3 fusion.11
  109.5 2.1 %gather_fusion = bf16[480,512]{1,0:T(8,128)(2,1)S(1)} fusion(bf16[193,512]{1,0:T(8,128)(2,1)S(1)} %concatenate.3, s32[1024]{0:T(1024)S(1)} %pad_clamp_fusion.1), kind=kCustom, calls=%fused_computation | custom fusion | bytes 984960 | tf_op jit(solution)/shard_map/jit(_take)/gather | solution.py:100
  111.6 0.1 gather.13
  111.7 0.1 broadcast_in_dim.65
  111.8 0.1 broadcast_select_fusion.1
  112.0 20.3 %all_to_all.21 = bf16[8,60,512]{2,1,0:T(8,128)(2,1)S(1)} all-to-all(bf16[8,60,512]{2,1,0:T(8,128)(2,1)S(1)} %broadcast_select_fusion.1), channel_id=1, replica_groups=mesh['sp'=8,'tp'=4] {'sp'}, dimensions={0} | all-to-all | bytes 983040 | tf_op jit(solution)/shard_map/all_to_all | solution.py:101
  132.3 0.9 all_to_all.7
  133.2 0.0 all-gather.2.cloned.1.call-update
  133.2 0.1 reduce_sum.53
  133.3 0.0 copy-start.10
  133.4 0.1 copy.70
  133.4 20.1 %all-gather.2.cloned.1.call-done = bf16[1,480,2048]{2,1,0:T(8,128)(2,1)} async-done(((bf16[1,480,512]{2,1,0:T(8,128)(2,1)}), bf16[1,480,2048]{2,1,0:T(8,128)(2,1)}) %all-gather.2.cloned.1.call-update) | async-done | bytes 1966096 | tf_op jit(solution)/shard_map/all_gather | solution.py:103
  153.6 2.7 %fusion.7 = f32[480,256]{1,0:T(8,128)S(1)} fusion(bf16[1,480,2048]{2,1,0:T(8,128)(2,1)} %all-gather.2.cloned.1.call-done, bf16[1,256,2048]{2,1,0:T(8,128)(2,1)} %param.26), kind=kOutput, calls=%fused_computation.12 | convolution fusion | flops 503316480 | bytes 3506176 | tf_op jit(solution)/shard_map/erd,efd->erf/dot_general | solution.py:104
  156.3 0.7 fusion.20
  157.0 0.0 copy-start.6
  157.0 9.8 %all_gather.27 = bf16[480,1024]{1,0:T(8,128)(2,1)S(1)} all-gather(bf16[480,256]{1,0:T(8,128)(2,1)S(1)} %fusion.20), channel_id=1, replica_groups=mesh['sp'=8,'tp'=4] {'tp'}, dimensions={1}, use_global_device_ids=true | all-gather | bytes 1228800 | tf_op jit(solution)/shard_map/all_gather | solution.py:110
  166.8 0.7 fusion.15
  167.5 0.8 copy.95
  168.3 0.6 broadcast.119
  168.9 3.7 %reduce.4 = bf16[480,512]{1,0:T(8,128)(2,1)S(1)} reduce(bf16[480,1,512]{2,1,0:T(2,128)(2,1)S(1)} %bitcast.81, bf16[]{:T(256)} %broadcast.119), dimensions={1}, to_apply=%bitcast.78.reduce_sub_computation | reduce | bytes 983042
  172.5 1.0 reshape.198
  173.5 5.5 %all-to-all-start.1 = ((bf16[8,2,15360]{2,1,0:T(2,128)(2,1)}), bf16[8,2,15360]{2,1,0:T(2,128)(2,1)S(1)}, u32[]{:S(2)}, u32[]{:S(2)}) async-start(bf16[8,2,15360]{2,1,0:T(2,128)(2,1)} %reshape.198), calls=%async_computation.1 | async-start | bytes 983040 | tf_op jit(solution)/shard_map/all_to_all | solution.py:118
  179.0 0.2 copy.71
  179.2 0.1 copy.74
  179.3 1.7 fusion.43
  181.1 1.7 fusion.25
  182.8 6.3 %all_gather.25 = bf16[192,1024]{1,0:T(8,128)(2,1)S(1)} all-gather(bf16[192,256]{1,0:T(8,128)(2,1)S(1)} %fusion.25), channel_id=1, replica_groups=mesh['sp'=8,'tp'=4] {'tp'}, dimensions={1}, use_global_device_ids=true | all-gather | bytes 491520 | tf_op jit(solution)/shard_map/all_gather | solution.py:109
  189.1 4.2 %all-to-all-done.1 = bf16[8,2,15360]{2,1,0:T(2,128)(2,1)S(1)} async-done(((bf16[8,2,15360]{2,1,0:T(2,128)(2,1)}), bf16[8,2,15360]{2,1,0:T(2,128)(2,1)S(1)}, u32[]{:S(2)}, u32[]{:S(2)}) %all-to-all-start.1) | async-done | bytes 491552 | tf_op jit(solution)/shard_map/all_to_all | solution.py:118
  193.3 0.4 reshape.199
  193.7 0.1 copy.94
  193.9 0.0 copy-start.1
  193.9 2.1 gather_fusion.1
  195.9 0.2 gather.15
  196.1 1.6 multiply_reduce_fusion
  197.7 2.0 fusion.24
  (35 shorter events, 0.2 us)
Async XLA Ops:
  6.5 160.3 %copy-start = (bf16[1,1024,512]{2,1,0:T(8,128)(2,1)S(1)}, bf16[1,1024,512]{2,1,0:T(8,128)(2,1)}, u32[]{:S(2)}) copy-start(bf16[1,1024,512]{2,1,0:T(8,128)(2,1)} %param.28) | copy-start | bytes 3145732
  6.5 147.0 %all-gather.2.cloned.1.call-start = ((), (), s32[]{:S(2)}) async-start(), calls=%async_computation.2 | async-start | bytes 2457600 | tf_op jit(solution)/shard_map/all_gather | solution.py:103
  50.5 4.5 %copy-start.2 = (bf16[192,256]{1,0:T(8,128)(2,1)S(1)}, bf16[192,256]{1,0:T(8,128)(2,1)}, u32[]{:S(2)}) copy-start(bf16[192,256]{1,0:T(8,128)(2,1)} %param.19) | copy-start | bytes 294916
  87.4 4.1 %copy-start.5 = (f32[4]{0:T(128)S(1)}, f32[4]{0:T(128)}, u32[]{:S(2)}) copy-start(f32[4]{0:T(128)} %param.20) | copy-start | bytes 52
  87.4 4.2 %copy-start.7 = (f32[64]{0:T(128)S(1)}, f32[64]{0:T(128)}, u32[]{:S(2)}) copy-start(f32[64]{0:T(128)} %param.21) | copy-start | bytes 772
  87.4 11.6 %copy-start.9 = (bf16[1024,512]{1,0:T(8,128)(2,1)S(1)}, bf16[1024,512]{1,0:T(8,128)(2,1)}, u32[]{:S(2)}) copy-start(bf16[1024,512]{1,0:T(8,128)(2,1)} %param.22) | copy-start | bytes 3145732
  87.4 11.5 %copy-start.11 = (bf16[192,512]{1,0:T(8,128)(2,1)S(1)}, bf16[192,512]{1,0:T(8,128)(2,1)}, u32[]{:S(2)}) copy-start(bf16[192,512]{1,0:T(8,128)(2,1)} %param.16) | copy-start | bytes 589828
  91.4 17.7 %copy-start.4 = (f32[2048]{0:T(1024)S(1)}, f32[2048]{0:T(1024)}, u32[]{:S(2)}) copy-start(f32[2048]{0:T(1024)} %param.23) | copy-start | bytes 24580
  133.3 22.9 %copy-start.10 = (bf16[1,256,2048]{2,1,0:T(8,128)(2,1)S(1)}, bf16[1,256,2048]{2,1,0:T(8,128)(2,1)}, u32[]{:S(2)}) copy-start(bf16[1,256,2048]{2,1,0:T(8,128)(2,1)} %param.27) | copy-start | bytes 3145732
  153.6 2.7 %copy-start.8 = (bf16[1,480,2048]{2,1,0:T(8,128)(2,1)S(1)}, bf16[1,480,2048]{2,1,0:T(8,128)(2,1)}, u32[]{:S(2)}) copy-start(bf16[1,480,2048]{2,1,0:T(8,128)(2,1)} %all-gather.2.cloned.1.call-done) | copy-start | bytes 5898244
  157.0 22.0 %copy-start.3 = (s32[192,2]{0,1:T(2,128)S(1)}, s32[192,2]{0,1:T(2,128)}, u32[]{:S(2)}) copy-start(s32[192,2]{0,1:T(2,128)} %param.24) | copy-start | bytes 4612
  157.0 22.2 %copy-start.6 = (f32[192,2]{0,1:T(2,128)S(1)}, f32[192,2]{0,1:T(2,128)}, u32[]{:S(2)}) copy-start(f32[192,2]{0,1:T(2,128)} %param.25) | copy-start | bytes 4612
  173.5 19.8 %all-to-all-start.1 = ((bf16[8,2,15360]{2,1,0:T(2,128)(2,1)}), bf16[8,2,15360]{2,1,0:T(2,128)(2,1)S(1)}, u32[]{:S(2)}, u32[]{:S(2)}) async-start(bf16[8,2,15360]{2,1,0:T(2,128)(2,1)} %reshape.198), calls=%async_computation.1 | async-start | bytes 983040 | tf_op jit(solution)/shard_map/all_to_all | solution.py:118
  193.9 3.9 %copy-start.1 = (bf16[1024,512]{1,0:T(8,128)(2,1)S(1)}, bf16[1024,512]{1,0:T(8,128)(2,1)}, u32[]{:S(2)}) copy-start(bf16[1024,512]{1,0:T(8,128)(2,1)} %param.31) | copy-start | bytes 3145732
Sparse Core Ops, SparseCore 0:
  133.3 20.2 all-gather.1
where the time goes:
time: 207 us
  blocking collectives  119 us (57%)
  waiting for transfers between devices  24.4 us (12%)
  matrix products  16.5 us (8%)
  local copies, waits for them, and re-layouts  15.1 us (7%)
  between operations  13.8 us (7%)
  other arithmetic  12.6 us (6%)
  starting transfers between devices  5.51 us (3%)
    all_gather x1, blocking collectives, body(): key_piece = lax.all_gather(key_rows, 'sp', axis=0, tiled=True)  34.1 us
    all_gather x1, blocking collectives, body(): value_piece = lax.all_gather(value_rows, 'sp', axis=0, tiled=True)  32.1 us
    all_to_all x1, blocking collectives, body(): lax.all_to_all(outgoing, 'sp', split_axis=0, concat_axis=1, tiled=True)  20.3 us
    all_gather x1, waiting for transfers between devices, body(): pieces = lax.all_gather(arrived, 'tp', axis=2, tiled=True)  20.1 us
    all_gather x1, blocking collectives, body(): lax.all_gather(expert_flat, 'tp', axis=1, tiled=True)  9.84 us
    all_gather x1, blocking collectives, body(): full_rows = lax.all_gather(hidden_state, 'tp', axis=1, tiled=True)  8.9 us
    all_gather x1, blocking collectives, body(): lax.all_gather(head_out, 'tp', axis=1, tiled=True)  7.21 us
    all_gather x1, blocking collectives, body(): lax.all_gather(shared_hidden, 'tp', axis=1, tiled=True)  6.29 us
  transfers between devices with their start and end apart: 2, of which 2 were waited for; matrix products, arithmetic and copies ran while one was open for 2% of the time, Pallas kernels for 0%

commit v1 on v0

--- a/solution.py
+++ b/solution.py
@@ -100,7 +100,12 @@
     outgoing = jnp.take(padded, slot_token, axis=0).reshape(experts_all, capacity, col_dev)
     arrived = lax.all_to_all(outgoing, "sp", split_axis=0, concat_axis=1, tiled=True)
     arrived_rows = arrived.shape[1]
-    pieces = lax.all_gather(arrived, "tp", axis=2, tiled=True)
+    ring = [arrived]
+    for hop in range(3):
+        ring.append(lax.ppermute(ring[-1], "tp", [(dev, (dev + 1) % 4) for dev in range(4)]))
+    pieces = jnp.roll(
+        jnp.concatenate(ring[::-1], axis=2), (lax.axis_index("tp") + 1) * ring[0].shape[2], axis=2
+    )
     gate_add = jnp.einsum("erd,efd->erf", pieces, expert_gate, preferred_element_type=jnp.float32)
     up_add = jnp.einsum("erd,efd->erf", pieces, expert_up, preferred_element_type=jnp.float32)
     expert_hidden = (jax.nn.silu(gate_add) * up_add).astype(jnp.bfloat16)

time: 207 us -> 196 us (0.947)
  between operations: 13.8 us -> 0.49 us
  waiting for transfers between devices: 24.4 us -> 28.7 us
    ppermute x0 -> x3, waiting for transfers between devices: none -> 24.6 us  [body(): lax.ppermute(ring[-1], 'tp', [(dev, (dev + 1) % 4) for dev in range(4)])]
    all_gather x1 -> x0, waiting for transfers between devices: 20.1 us -> none  [body(): pieces = lax.all_gather(arrived, 'tp', axis=2, tiled=True)]
    unnamed x31 -> x38, local copies, waits for them, and re-layouts: 4.14 us -> 6.92 us
  transfers between devices with their start and end apart: 2 -> 4, of which waited for: 2 -> 4; matrix products, arithmetic and copies ran while one was open for 2% -> 2% of each run, Pallas kernels for 0% -> 0%
where the time goes in v1:
time: 196 us; the launch traced here: 195 us
  blocking collectives  118 us (60%)
  waiting for transfers between devices  28.7 us (15%)
  local copies, waits for them, and re-layouts  17.1 us (9%)
  matrix products  14.5 us (7%)
  other arithmetic  12.6 us (6%)
  starting transfers between devices  3.7 us (2%)
    all_gather x1, blocking collectives, body(): key_piece = lax.all_gather(key_rows, 'sp', axis=0, tiled=True)  34.1 us
    all_gather x1, blocking collectives, body(): value_piece = lax.all_gather(value_rows, 'sp', axis=0, tiled=True)  32.1 us
    ppermute x3, waiting for transfers between devices, body(): lax.ppermute(ring[-1], 'tp', [(dev, (dev + 1) % 4) for dev in range(4)])  24.6 us
    all_to_all x1, blocking collectives, body(): lax.all_to_all(outgoing, 'sp', split_axis=0, concat_axis=1, tiled=True)  20.3 us
    all_gather x1, blocking collectives, body(): lax.all_gather(expert_flat, 'tp', axis=1, tiled=True)  8.99 us
    all_gather x1, blocking collectives, body(): full_rows = lax.all_gather(hidden_state, 'tp', axis=1, tiled=True)  8.91 us
    all_gather x1, blocking collectives, body(): lax.all_gather(head_out, 'tp', axis=1, tiled=True)  7.19 us
    unnamed x38, local copies, waits for them, and re-layouts  6.92 us
  transfers between devices with their start and end apart: 4, of which 4 were waited for; matrix products, arithmetic and copies ran while one was open for 2% of the time, Pallas kernels for 0%

profile of v1, /device:TPU:0, one launch (start us, length us, event | category | flops | bytes accessed | tf_op | source)
XLA Modules:
  0.0 195.2 jit_solution(17674878508784875244)
XLA Ops:
  0.0 0.9 copy.68
  0.9 0.1 eq.29
  1.0 0.1 reshape.160
  1.2 0.7 broadcast_multiply_fusion
  1.9 0.8 reduce-window.6
  2.7 0.2 slice_reduce_fusion
  3.0 0.1 copy.72
  3.1 0.1 mul.127
  3.3 0.1 reshape.188
  3.4 0.1 fusion.34
  3.5 2.9 %scatter_custom_fusion = s32[480]{0:T(512)S(1)} fusion(s32[384]{0:T(512)S(1)} %fusion.36, s32[384]{0:T(512)S(1)} %reshape.188, s32[]{:T(128)} %constant.51.clone.1), kind=kCustom, calls=%fused_computation.75 | custom fusion | bytes 1924 | tf_op jit(solution)/shard_map/scatter | solution.py:96
  6.5 0.2 iota_compare_fusion
  6.7 34.1 %all_gather.18 = bf16[1536,256]{1,0:T(8,128)(2,1)S(1)} all-gather(bf16[192,256]{1,0:T(8,128)(2,1)} %param.18), channel_id=1, replica_groups=mesh['sp'=8,'tp'=4] {'sp'}, dimensions={0}, use_global_device_ids=true | all-gather | bytes 884736 | tf_op jit(solution)/shard_map/all_gather | solution.py:55
  40.8 0.3 copy.61
  41.1 1.0 copy.60
  42.1 1.9 fusion
  44.0 4.4 %fusion.1 = (f32[2,4,192]{2,1,0:T(4,128)S(1)}, bf16[2,4,192,1536]{3,2,1,0:T(8,128)(2,1)}) fusion(f32[2,4,192,1536]{3,2,1,0:T(8,128)S(1)} %get-tuple-element.8, f32[2,4,192]{2,1,0:T(4,128)S(1)} %broadcast_maximum_fusion, pred[192,1536]{1,0:T(8,128)(4,1)S(1)} %iota_compare_fusion), kind=kLoop, calls=%fused_computation.6 | loop fusion | flops 14154240 | bytes 14462976 | tf_op jit(solution)/shard_map/reduce_sum | solution.py:70
  48.4 32.1 %all_gather.19 = bf16[1536,256]{1,0:T(8,128)(2,1)S(1)} all-gather(bf16[192,256]{1,0:T(8,128)(2,1)S(1)} %copy-done.2), channel_id=1, replica_groups=mesh['sp'=8,'tp'=4] {'sp'}, dimensions={0}, use_global_device_ids=true | all-gather | bytes 884736 | tf_op jit(solution)/shard_map/all_gather | solution.py:56
  80.5 0.3 copy.64
  80.9 4.0 %fusion.25 = f32[2,4,192,64]{2,3,0,1:T(8,128)S(1)} fusion(bf16[1536,4,64,1]{0,2,3,1:T(8,128)(2,1)S(1)} %bitcast.84, bf16[2,4,192,1536]{3,2,1,0:T(8,128)(2,1)} %get-tuple-element.6, f32[2,4,192]{2,0,1:T(2,128)S(1)} %copy.66), kind=kOutput, calls=%fused_computation.35 | convolution fusion | flops 302088192 | bytes 5904384 | tf_op jit(solution)/shard_map/mhqk,khd->mhqd/dot_general | solution.py:71
  84.9 0.1 multiply_reduce_fusion.1
  85.1 0.1 multiply_convert_fusion.1
  85.2 7.2 %all_gather.20 = bf16[192,1024]{0,1:T(8,128)(2,1)S(1)} all-gather(bf16[192,256]{0,1:T(8,128)(2,1)S(1)} %bitcast.85), channel_id=1, replica_groups=mesh['sp'=8,'tp'=4] {'tp'}, dimensions={1}, use_global_device_ids=true | all-gather | bytes 491520 | tf_op jit(solution)/shard_map/all_gather | solution.py:79
  92.4 1.1 fusion.19
  93.5 8.9 %all_gather.21 = bf16[192,2048]{1,0:T(8,128)(2,1)S(1)} all-gather(bf16[192,512]{1,0:T(8,128)(2,1)} %fusion.19), channel_id=1, replica_groups=mesh['sp'=8,'tp'=4] {'tp'}, dimensions={1}, use_global_device_ids=true | all-gather | bytes 983040 | tf_op jit(solution)/shard_map/all_gather | solution.py:84
  102.4 0.2 fusion.11
  102.7 0.3 fusion.13
  103.0 2.1 %gather_fusion = bf16[480,512]{1,0:T(8,128)(2,1)S(1)} fusion(bf16[193,512]{1,0:T(8,128)(2,1)S(1)} %concatenate.9, s32[1024]{0:T(1024)S(1)} %get-tuple-element.10), kind=kCustom, calls=%fused_computation | custom fusion | bytes 984960 | tf_op jit(solution)/shard_map/jit(_take)/gather | solution.py:100
  105.1 0.1 gather.13
  105.2 0.1 broadcast_in_dim.65
  105.3 0.1 broadcast_select_fusion.1
  105.4 20.3 %all_to_all.21 = bf16[8,60,512]{2,1,0:T(8,128)(2,1)S(1)} all-to-all(bf16[8,60,512]{2,1,0:T(8,128)(2,1)S(1)} %broadcast_select_fusion.1), channel_id=1, replica_groups=mesh['sp'=8,'tp'=4] {'sp'}, dimensions={0} | all-to-all | bytes 983040 | tf_op jit(solution)/shard_map/all_to_all | solution.py:101
  125.7 0.1 all_to_all.7
  125.8 0.1 collective-permute-start
  125.9 8.2 %collective-permute-done = bf16[1,480,512]{2,1,0:T(8,128)(2,1)S(1)} collective-permute-done((bf16[1,480,512]{2,1,0:T(8,128)(2,1)S(1)}, bf16[1,480,512]{2,1,0:T(8,128)(2,1)S(1)}, u32[]{:S(2)}, u32[]{:S(2)}) %collective-permute-start) | collective-permute-done | bytes 491552 | tf_op jit(solution)/shard_map/ppermute | solution.py:105
  134.1 8.3 %collective-permute-done.1 = bf16[1,480,512]{2,1,0:T(8,128)(2,1)S(1)} collective-permute-done((bf16[1,480,512]{2,1,0:T(8,128)(2,1)S(1)}, bf16[1,480,512]{2,1,0:T(8,128)(2,1)S(1)}, u32[]{:S(2)}, u32[]{:S(2)}) %collective-permute-start.1) | collective-permute-done | bytes 491552 | tf_op jit(solution)/shard_map/ppermute | solution.py:105
  142.4 0.1 reduce_sum.53
  142.6 0.1 copy.70
  142.6 8.1 %collective-permute-done.2 = bf16[1,480,512]{2,1,0:T(8,128)(2,1)} collective-permute-done((bf16[1,480,512]{2,1,0:T(8,128)(2,1)S(1)}, bf16[1,480,512]{2,1,0:T(8,128)(2,1)}, u32[]{:S(2)}, u32[]{:S(2)}) %collective-permute-start.2) | collective-permute-done | bytes 491552 | tf_op jit(solution)/shard_map/ppermute | solution.py:105
  150.8 1.1 constant_dynamic-update-slice_fusion.7
  151.8 0.1 constant_dynamic-update-slice_fusion.6
  152.0 1.1 constant_dynamic-update-slice_fusion.3
  153.3 0.7 fusion.7
  154.0 0.4 copy-done.10
  154.4 0.7 multiply_convert_fusion
  155.1 9.0 %all_gather.23 = bf16[480,1024]{1,0:T(8,128)(2,1)S(1)} all-gather(bf16[480,256]{1,0:T(8,128)(2,1)S(1)} %multiply_convert_fusion), channel_id=1, replica_groups=mesh['sp'=8,'tp'=4] {'tp'}, dimensions={1}, use_global_device_ids=true | all-gather | bytes 1228800 | tf_op jit(solution)/shard_map/all_gather | solution.py:115
  164.1 0.7 fusion.17
  164.8 0.8 copy.95
  165.6 0.6 broadcast.120
  166.2 3.7 %reduce.4 = bf16[480,512]{1,0:T(8,128)(2,1)S(1)} reduce(bf16[480,1,512]{2,1,0:T(2,128)(2,1)S(1)} %bitcast.81, bf16[]{:T(256)} %broadcast.120), dimensions={1}, to_apply=%bitcast.78.reduce_sub_computation | reduce | bytes 983042
  169.8 1.0 reshape.198
  170.8 3.6 %all-to-all-start.1 = ((bf16[8,2,15360]{2,1,0:T(2,128)(2,1)}), bf16[8,2,15360]{2,1,0:T(2,128)(2,1)S(1)}, u32[]{:S(2)}, u32[]{:S(2)}) async-start(bf16[8,2,15360]{2,1,0:T(2,128)(2,1)} %reshape.198), calls=%async_computation.1 | async-start | bytes 983040 | tf_op jit(solution)/shard_map/all_to_all | solution.py:123
  174.5 0.2 copy.71
  174.6 0.1 copy.74
  174.8 1.7 fusion.45
  176.5 1.7 fusion.21
  178.2 6.4 %all_gather.22 = bf16[192,1024]{1,0:T(8,128)(2,1)S(1)} all-gather(bf16[192,256]{1,0:T(8,128)(2,1)S(1)} %fusion.21), channel_id=1, replica_groups=mesh['sp'=8,'tp'=4] {'tp'}, dimensions={1}, use_global_device_ids=true | all-gather | bytes 491520 | tf_op jit(solution)/shard_map/all_gather | solution.py:114
  184.7 4.1 %all-to-all-done.1 = bf16[8,2,15360]{2,1,0:T(2,128)(2,1)S(1)} async-done(((bf16[8,2,15360]{2,1,0:T(2,128)(2,1)}), bf16[8,2,15360]{2,1,0:T(2,128)(2,1)S(1)}, u32[]{:S(2)}, u32[]{:S(2)}) %all-to-all-start.1) | async-done | bytes 491552 | tf_op jit(solution)/shard_map/all_to_all | solution.py:123
  188.8 0.4 reshape.199
  189.2 0.1 copy.94
  189.3 2.1 %gather_fusion.1 = bf16[384,512]{1,0:T(8,128)(2,1)S(1)} fusion(bf16[480,512]{1,0:T(8,128)(2,1)S(1)} %bitcast.80, s32[1024]{0:T(1024)S(1)} %get-tuple-element.9), kind=kCustom, calls=%fused_computation.1 | custom fusion | bytes 787968 | tf_op jit(solution)/shard_map/jit(_take)/gather | solution.py:128
  191.4 0.2 gather.15
  191.6 1.6 multiply_reduce_fusion
  193.2 2.0 %fusion.20 = bf16[192,512]{1,0:T(8,128)(2,1)} fusion(f32[192,512]{1,0:T(8,128)S(1)} %multiply_reduce_fusion, bf16[192,1024]{1,0:T(8,128)(2,1)S(1)} %all_gather.22, bf16[1024,512]{1,0:T(8,128)(2,1)S(1)} %copy-done.1, bf16[192,512]{1,0:T(8,128)(2,1)} %fusion.19), kind=kOutput, calls=%fused_computation.29 | convolution fusion | flops 201719808 | bytes 2228224 | tf_op jit(solution)/shard_map/dot_general | solution.py:119
  (45 shorter events, 0.5 us)
Async XLA Ops:
  0.0 164.1 %copy-start = (bf16[1,1024,512]{2,1,0:T(8,128)(2,1)S(1)}, bf16[1,1024,512]{2,1,0:T(8,128)(2,1)}, u32[]{:S(2)}) copy-start(bf16[1,1024,512]{2,1,0:T(8,128)(2,1)} %param.28) | copy-start | bytes 3145732
  44.0 4.5 %copy-start.2 = (bf16[192,256]{1,0:T(8,128)(2,1)S(1)}, bf16[192,256]{1,0:T(8,128)(2,1)}, u32[]{:S(2)}) copy-start(bf16[192,256]{1,0:T(8,128)(2,1)} %param.19) | copy-start | bytes 294916
  80.8 4.1 %copy-start.5 = (f32[4]{0:T(128)S(1)}, f32[4]{0:T(128)}, u32[]{:S(2)}) copy-start(f32[4]{0:T(128)} %param.20) | copy-start | bytes 52
  80.8 4.2 %copy-start.7 = (f32[64]{0:T(128)S(1)}, f32[64]{0:T(128)}, u32[]{:S(2)}) copy-start(f32[64]{0:T(128)} %param.21) | copy-start | bytes 772
  80.8 11.5 %copy-start.8 = (bf16[1024,512]{1,0:T(8,128)(2,1)S(1)}, bf16[1024,512]{1,0:T(8,128)(2,1)}, u32[]{:S(2)}) copy-start(bf16[1024,512]{1,0:T(8,128)(2,1)} %param.22) | copy-start | bytes 3145732
  80.9 11.5 %copy-start.11 = (bf16[192,512]{1,0:T(8,128)(2,1)S(1)}, bf16[192,512]{1,0:T(8,128)(2,1)}, u32[]{:S(2)}) copy-start(bf16[192,512]{1,0:T(8,128)(2,1)} %param.16) | copy-start | bytes 589828
  84.9 17.7 %copy-start.4 = (f32[2048]{0:T(1024)S(1)}, f32[2048]{0:T(1024)}, u32[]{:S(2)}) copy-start(f32[2048]{0:T(1024)} %param.23) | copy-start | bytes 24580
  125.8 8.3 %collective-permute-start = (bf16[1,480,512]{2,1,0:T(8,128)(2,1)S(1)}, bf16[1,480,512]{2,1,0:T(8,128)(2,1)S(1)}, u32[]{:S(2)}, u32[]{:S(2)}) collective-permute-start(bf16[1,480,512]{2,1,0:T(8,128)(2,1)S(1)} %all_to_all.7), channel_id=1, source_target_pairs={{0,1},{1,2},{2,3},{3,0},{4,5},{5,6},{6,7},{7,4},{8,9},{9,10},{10,1... | collective-permute-start | bytes 1474568 | tf_op jit(solution)/shard_map/ppermute | solution.py:105
  134.1 8.3 %collective-permute-start.1 = (bf16[1,480,512]{2,1,0:T(8,128)(2,1)S(1)}, bf16[1,480,512]{2,1,0:T(8,128)(2,1)S(1)}, u32[]{:S(2)}, u32[]{:S(2)}) collective-permute-start(bf16[1,480,512]{2,1,0:T(8,128)(2,1)S(1)} %collective-permute-done), channel_id=1, source_target_pairs={{0,1},{1,2},{2,3},{3,0},{4,5},{5,6},{6,7},{7,4},{8,9},{9,10},{10,1... | collective-permute-start | bytes 1474568 | tf_op jit(solution)/shard_map/ppermute | solution.py:105
  142.4 8.4 %collective-permute-start.2 = (bf16[1,480,512]{2,1,0:T(8,128)(2,1)S(1)}, bf16[1,480,512]{2,1,0:T(8,128)(2,1)}, u32[]{:S(2)}, u32[]{:S(2)}) collective-permute-start(bf16[1,480,512]{2,1,0:T(8,128)(2,1)S(1)} %collective-permute-done.1), channel_id=1, source_target_pairs={{0,1},{1,2},{2,3},{3,0},{4,5},{5,6},{6,7},{7,4},{8,9},{9,10},{10,1... | collective-permute-start | bytes 1474568 | tf_op jit(solution)/shard_map/ppermute | solution.py:105
  142.6 10.7 %copy-start.9 = (bf16[1,256,2048]{2,1,0:T(8,128)(2,1)S(1)}, bf16[1,256,2048]{2,1,0:T(8,128)(2,1)}, u32[]{:S(2)}) copy-start(bf16[1,256,2048]{2,1,0:T(8,128)(2,1)} %param.26) | copy-start | bytes 3145732
  153.2 1.2 copy-start.10
  164.1 10.3 %copy-start.3 = (s32[192,2]{0,1:T(2,128)S(1)}, s32[192,2]{0,1:T(2,128)}, u32[]{:S(2)}) copy-start(s32[192,2]{0,1:T(2,128)} %param.24) | copy-start | bytes 4612
  164.1 10.5 %copy-start.6 = (f32[192,2]{0,1:T(2,128)S(1)}, f32[192,2]{0,1:T(2,128)}, u32[]{:S(2)}) copy-start(f32[192,2]{0,1:T(2,128)} %param.25) | copy-start | bytes 4612
  170.8 18.0 %all-to-all-start.1 = ((bf16[8,2,15360]{2,1,0:T(2,128)(2,1)}), bf16[8,2,15360]{2,1,0:T(2,128)(2,1)S(1)}, u32[]{:S(2)}, u32[]{:S(2)}) async-start(bf16[8,2,15360]{2,1,0:T(2,128)(2,1)} %reshape.198), calls=%async_computation.1 | async-start | bytes 983040 | tf_op jit(solution)/shard_map/all_to_all | solution.py:123
  189.3 3.9 %copy-start.1 = (bf16[1024,512]{1,0:T(8,128)(2,1)S(1)}, bf16[1024,512]{1,0:T(8,128)(2,1)}, u32[]{:S(2)}) copy-start(bf16[1024,512]{1,0:T(8,128)(2,1)} %param.31) | copy-start | bytes 3145732
